TPU v7x, 32 devices: a whole 2x2x4 slice. The times are simulated.
32 devices in a mesh: ep: 8 (over z, core), tp: 4 (over y, x).
Axes of the slice: x: 2, y: 2, z: 4, core: 2. Of those that a mesh axis runs over, the one named last changes fastest.
Arguments:
- tokens: bfloat16 [1024, 1024], P('ep', 'tp'), may hold values from -6 to 6
- norm_gain: float32 [1024], replicated, may hold values from 0.1 to 1.9
- gate_weight: bfloat16 [8, 1024, 1024], P('ep', None, 'tp'), may hold values from -0.1875 to 0.1875
- up_weight: bfloat16 [8, 1024, 1024], P('ep', None, 'tp'), may hold values from -0.1875 to 0.1875
- down_weight: bfloat16 [8, 1024, 1024], P('ep', None, 'tp'), may hold values from -0.1875 to 0.1875
- expert_ids: int32 [1024, 4], P('ep'), may hold values from 0 to 7, all different within a row; in each aligned block of 128 rows (0 to 127, 128 to 255, ...) at most 128 rows name the same one
- route_weight: float32 [1024, 4], P('ep'), may hold values from 0.2 to 1
Outputs:
- combined: bfloat16 [1024, 1024], P('ep', 'tp')
Inputs may be any that keep to these rules, and one draw needn't show every extreme that they name: `expert_ids`: each token names 4 different experts; in each aligned block of 128 tokens no expert is named by more than 128 of them, and in some block one expert is named by exactly 128; every expert is named by some token.
All inputs are finite; a program needn't handle non-finite values.
Results may differ from a plain program's by a relative error of at most 0.0035.
Values may be sent and summed in bfloat16 or wider, within the bound.
A program may use at most 64 MiB of HBM per device.

v0:
```python
import jax
import jax.numpy as jnp
from jax import lax
from jax.sharding import PartitionSpec as P

epsilon = 1e-06
swish_alpha = 1.702
clamp_limit = 7.0


def over_all(shard, axis, dim, take_in, carry):
    whole = jax.tree.map(lambda part: lax.all_gather(part, axis, axis=dim, tiled=True), shard)
    return take_in(carry, whole, jnp.int32(0))


def rms_normed(values, norm_gain):
    widened = values.astype(jnp.float32)
    scaled = widened * lax.rsqrt(jnp.mean(widened * widened, axis=-1, keepdims=True) + epsilon)
    return (scaled * norm_gain.astype(jnp.float32)).astype(jnp.bfloat16)


def slot_numbers(flat_ids, expert_count):
    selector = (flat_ids[..., None] == jnp.arange(expert_count, dtype=jnp.int32)).astype(jnp.int32)
    before = jnp.cumsum(selector, axis=-2) - selector
    return jnp.sum(before * selector, axis=-1).astype(jnp.int32)


def by_expert(incoming, ep_count, local_experts):
    capacity = incoming.shape[1]
    width = incoming.shape[2]
    grouped = incoming.reshape(ep_count, local_experts, capacity, width)
    return jnp.transpose(grouped, (1, 0, 2, 3)).reshape(local_experts, ep_count * capacity, width)


def body(tokens, norm_gain, gate_weight, up_weight, down_weight, expert_ids, route_weight):
    tok_rows = expert_ids.shape[0]
    top_count = expert_ids.shape[1]
    local_experts = gate_weight.shape[0]
    ep_count = lax.axis_size("ep")
    expert_total = local_experts * ep_count
    capacity = 2 * tok_rows * top_count // expert_total
    out_width = down_weight.shape[2]
    flat_ids = expert_ids.reshape(-1).astype(jnp.int32)
    slot_index = slot_numbers(flat_ids, expert_total)
    owner_token = jnp.arange(tok_rows * top_count, dtype=jnp.int32) // top_count
    slot_table = (
        jnp.full((expert_total, capacity), tok_rows, jnp.int32)
        .at[flat_ids, slot_index]
        .set(owner_token)
    )
    whole = lax.all_gather(tokens, "tp", axis=1, tiled=True)
    normed = rms_normed(whole, norm_gain)
    width = normed.shape[1]
    padded = jnp.concatenate([normed, jnp.zeros((1, width), jnp.bfloat16)], axis=0)
    outgoing = padded[slot_table.reshape(-1)].reshape(expert_total, capacity, width)
    incoming = lax.all_to_all(outgoing, "ep", split_axis=0, concat_axis=0, tiled=True)
    row_block = by_expert(incoming, ep_count, local_experts)
    gate_pre = jnp.einsum(
        "esd,edf->esf", row_block, gate_weight, preferred_element_type=jnp.float32
    )
    up_pre = jnp.einsum("esd,edf->esf", row_block, up_weight, preferred_element_type=jnp.float32)
    gate_pre = jnp.minimum(gate_pre, clamp_limit)
    up_pre = jnp.clip(up_pre, -clamp_limit, clamp_limit)
    hidden = ((up_pre + 1.0) * gate_pre * jax.nn.sigmoid(swish_alpha * gate_pre)).astype(
        jnp.bfloat16
    )
    empty_out = jnp.zeros((local_experts, ep_count * capacity, out_width), jnp.float32)

    def add_hidden(total, piece, start):
        down_rows = lax.dynamic_slice_in_dim(down_weight, start, piece.shape[2], 1)
        return total + jnp.einsum(
            "esf,efd->esd", piece, down_rows, preferred_element_type=jnp.float32
        )

    down_sum = over_all(hidden, "tp", 2, add_hidden, empty_out)
    expert_out = down_sum.astype(jnp.bfloat16).reshape(local_experts, ep_count, capacity, out_width)
    sendback = jnp.transpose(expert_out, (1, 0, 2, 3)).reshape(
        ep_count * local_experts, capacity, out_width
    )
    returned = lax.all_to_all(sendback, "ep", split_axis=0, concat_axis=0, tiled=True)
    flat_back = returned.reshape(expert_total * capacity, out_width)
    picked = (
        flat_back[flat_ids * capacity + slot_index]
        .reshape(tok_rows, top_count, out_width)
        .astype(jnp.float32)
    )
    combined = jnp.sum(picked * route_weight.astype(jnp.float32)[:, :, None], axis=1)
    return combined.astype(jnp.bfloat16)


def solution(mesh):
    in_specs = (
        P("ep", "tp"),
        P(),
        P("ep", None, "tp"),
        P("ep", None, "tp"),
        P("ep", None, "tp"),
        P("ep", None),
        P("ep", None),
    )
    out_specs = P("ep", "tp")
    return jax.shard_map(body, mesh=mesh, in_specs=in_specs, out_specs=out_specs, check_vma=False)
```

profile of v0, /device:TPU:0, one launch (start us, length us, event | category | flops | bytes accessed | tf_op | source)
XLA Modules:
  0.0 170.0 jit_solution(460344144802858195)
XLA Ops:
  6.5 0.0 copy-start
  6.5 0.0 all-gather.3.cloned.1.call-start
  6.5 0.8 copy.9
  7.4 0.1 eq.29
  7.5 0.1 eq.25
  7.6 0.1 reshape.171
  7.7 1.1 reduce-window.6
  8.9 0.2 slice_reduce_fusion
  9.1 0.1 fusion.11
  9.3 0.0 copy-start.1
  9.3 0.0 copy-start.2
  9.3 22.1 %scatter_fusion = s32[8,128]{1,0:T(8,128)S(1)} fusion(s32[8,128]{1,0:T(8,128)S(1)} %broadcast_in_dim.2, s32[512]{0:T(512)S(1)} %bitcast.30, s32[512]{0:T(512)S(1)} %add_select_fusion), kind=kCustom, calls=%fused_computation.2 | custom fusion | bytes 10240 | tf_op jit(solution)/shard_map/scatter | solution.py:49
  31.4 0.0 copy-done.1
  31.4 11.6 %all_gather.6 = bf16[128,1024]{1,0:T(8,128)(2,1)S(1)} all-gather(bf16[128,256]{1,0:T(8,128)(2,1)S(1)} %copy-done.1), channel_id=1, replica_groups=mesh['ep'=8,'tp'=4] {'tp'}, dimensions={1}, use_global_device_ids=true | all-gather | bytes 327680 | tf_op jit(solution)/shard_map/all_gather | solution.py:51
  43.0 0.1 fusion.4
  43.1 0.0 copy-done.2
  43.1 0.1 fusion.6
  43.3 4.1 %gather_fusion = bf16[1024,1024]{1,0:T(8,128)(2,1)S(1)} fusion(bf16[129,1024]{1,0:T(8,128)(2,1)S(1)} %concatenate.6, s32[1024]{0:T(1024)S(1)} %broadcast_clamp_fusion), kind=kCustom, calls=%fused_computation | custom fusion | bytes 4198400 | tf_op jit(solution)/shard_map/gather | solution.py:55
  47.4 53.8 %all_to_all.10 = bf16[8,128,1024]{2,1,0:T(8,128)(2,1)S(1)} all-to-all(bf16[8,128,1024]{2,1,0:T(8,128)(2,1)S(1)} %bitcast.32), channel_id=1, replica_groups=mesh['ep'=8,'tp'=4] {'ep'}, dimensions={0} | all-to-all | bytes 4194304 | tf_op jit(solution)/shard_map/all_to_all | solution.py:56
  101.2 0.7 convolution_minimum_fusion
  101.9 0.3 copy-done.4
  102.2 1.6 fusion.3
  103.8 0.0 all-gather.3.cloned.1.call-update
  103.8 0.0 copy-start.3
  103.9 33.0 %all-gather.3.cloned.1.call-done = bf16[1024,1024]{1,0:T(8,128)(2,1)} async-done(((bf16[1024,256]{1,0:T(8,128)(2,1)}), bf16[1024,1024]{1,0:T(8,128)(2,1)}) %all-gather.3.cloned.1.call-update) | async-done | bytes 2097168 | tf_op jit(solution)/shard_map/all_gather | solution.py:12
  136.9 3.1 %convolution_convert_fusion = bf16[1024,256]{1,0:T(8,128)(2,1)} fusion(bf16[1024,1024]{1,0:T(8,128)(2,1)} %all-gather.3.cloned.1.call-done, bf16[1,1024,256]{2,1,0:T(8,128)(2,1)S(1)} %copy-done.5), kind=kOutput, calls=%fused_computation.8 | convolution fusion | flops 537133056 | bytes 3145728 | tf_op jit(solution)/shard_map/esf,efd->esd/dot_general | solution.py:71
  140.0 4.6 %all-to-all-start.1 = ((bf16[8,128,256]{2,1,0:T(8,128)(2,1)}), bf16[8,128,256]{2,1,0:T(8,128)(2,1)S(1)}, u32[]{:S(2)}, u32[]{:S(2)}) async-start(bf16[8,128,256]{2,1,0:T(8,128)(2,1)} %bitcast.11), calls=%async_computation.1 | async-start | bytes 1048576 | tf_op jit(solution)/shard_map/all_to_all | solution.py:80
  144.6 0.1 copy.12
  144.7 15.3 %all-to-all-done.1 = bf16[8,128,256]{2,1,0:T(8,128)(2,1)S(1)} async-done(((bf16[8,128,256]{2,1,0:T(8,128)(2,1)}), bf16[8,128,256]{2,1,0:T(8,128)(2,1)S(1)}, u32[]{:S(2)}, u32[]{:S(2)}) %all-to-all-start.1) | async-done | bytes 524320 | tf_op jit(solution)/shard_map/all_to_all | solution.py:80
  160.0 1.9 %gather_fusion.1 = bf16[512,256]{1,0:T(8,128)(2,1)S(1)} fusion(bf16[1024,256]{1,0:T(8,128)(2,1)S(1)} %bitcast.31, s32[1024]{0:T(1024)S(1)} %pad_clamp_fusion), kind=kCustom, calls=%fused_computation.1 | custom fusion | bytes 526336 | tf_op jit(solution)/shard_map/gather | solution.py:83
  162.0 0.1 reshape.181
  162.1 1.0 multiply_reduce_fusion
  (16 shorter events, 0.1 us)
Async XLA Ops:
  6.5 94.6 %copy-start = (bf16[1,1024,256]{2,1,0:T(8,128)(2,1)S(1)}, bf16[1,1024,256]{2,1,0:T(8,128)(2,1)}, u32[]{:S(2)}) copy-start(bf16[1,1024,256]{2,1,0:T(8,128)(2,1)} %param.9) | copy-start | bytes 1572868
  6.5 130.4 %all-gather.3.cloned.1.call-start = ((), (), s32[]{:S(2)}) async-start(), calls=%async_computation.2 | async-start | bytes 2621440 | tf_op jit(solution)/shard_map/all_gather | solution.py:12
  9.3 22.1 %copy-start.1 = (bf16[128,256]{1,0:T(8,128)(2,1)S(1)}, bf16[128,256]{1,0:T(8,128)(2,1)}, u32[]{:S(2)}) copy-start(bf16[128,256]{1,0:T(8,128)(2,1)} %param.7) | copy-start | bytes 196612
  9.3 33.8 %copy-start.2 = (f32[1024]{0:T(1024)S(1)}, f32[1024]{0:T(1024)}, u32[]{:S(2)}) copy-start(f32[1024]{0:T(1024)} %param.8) | copy-start | bytes 12292
  101.2 1.0 copy-start.4
  102.2 34.7 %copy-start.5 = (bf16[1,1024,256]{2,1,0:T(8,128)(2,1)S(1)}, bf16[1,1024,256]{2,1,0:T(8,128)(2,1)}, u32[]{:S(2)}) copy-start(bf16[1,1024,256]{2,1,0:T(8,128)(2,1)} %param.11) | copy-start | bytes 1572868
  103.8 40.8 %copy-start.3 = (f32[128,4]{0,1:T(4,128)S(1)}, f32[128,4]{0,1:T(4,128)}, u32[]{:S(2)}) copy-start(f32[128,4]{0,1:T(4,128)} %param.13) | copy-start | bytes 6148
  140.0 20.0 %all-to-all-start.1 = ((bf16[8,128,256]{2,1,0:T(8,128)(2,1)}), bf16[8,128,256]{2,1,0:T(8,128)(2,1)S(1)}, u32[]{:S(2)}, u32[]{:S(2)}) async-start(bf16[8,128,256]{2,1,0:T(8,128)(2,1)} %bitcast.11), calls=%async_computation.1 | async-start | bytes 1048576 | tf_op jit(solution)/shard_map/all_to_all | solution.py:80
Sparse Core Ops, SparseCore 0:
  104.0 32.8 all-gather.2
where the time goes:
time: 170 us
  blocking collectives  65.3 us (38%)
  waiting for transfers between devices  48.3 us (28%)
  local copies, waits for them, and re-layouts  30.1 us (18%)
  between operations  13.5 us (8%)
  matrix products  5.44 us (3%)
  starting transfers between devices  4.61 us (3%)
  other arithmetic  2.63 us (2%)
    all_to_all x1, blocking collectives, body(): lax.all_to_all(outgoing, 'ep', split_axis=0, concat_axis=0, tiled=True)  53.8 us
    all_gather x1, waiting for transfers between devices, over_all(): lax.all_gather(part, axis, axis=dim, tiled=True)  33 us
    scatter x1, local copies, waits for them, and re-layouts, body(): slot_table = jnp.full((expert_total, capacity), tok_rows, jnp.int32).at[f...  22.1 us
    all_to_all x1, waiting for transfers between devices, body(): lax.all_to_all(sendback, 'ep', split_axis=0, concat_axis=0, tiled=True)  15.3 us
    all_gather x1, blocking collectives, body(): whole = lax.all_gather(tokens, 'tp', axis=1, tiled=True)  11.6 us
    all_to_all x1, starting transfers between devices, body(): lax.all_to_all(sendback, 'ep', split_axis=0, concat_axis=0, tiled=True)  4.61 us
    gather x1, local copies, waits for them, and re-layouts, body(): padded[slot_table.reshape(-1)].reshape(expert_total, capacity, width)  4.07 us
  transfers between devices with their start and end apart: 2, of which 2 were waited for; matrix products, arithmetic and copies ran while one was open for 0% of the time, Pallas kernels for 0%

commit v1 on v0

--- a/solution.py
+++ b/solution.py
@@ -1,6 +1,10 @@
+import functools
+
 import jax
 import jax.numpy as jnp
 from jax import lax
+from jax.experimental import pallas as pl
+from jax.experimental.pallas import tpu as pltpu
 from jax.sharding import PartitionSpec as P
 
 epsilon = 1e-06
@@ -88,6 +92,364 @@
     return combined.astype(jnp.bfloat16)
 
 
+MESH = pl.DeviceIdType.MESH
+
+
+def fused_kernel(
+    nz,
+    gain_ref,
+    ids_ref,
+    route_ref,
+    tok_ref,
+    gw_ref,
+    uw_ref,
+    dw_ref,
+    out_ref,
+    xbuf,
+    gw,
+    uw,
+    wd,
+    nbuf,
+    wbuf,
+    keep,
+    dsend,
+    drecv,
+    r1send,
+    r1recv,
+    r2send,
+    r2recv,
+    zsend,
+    zrecv,
+    near,
+    lsem,
+    wd_s,
+    wd_r,
+    w_s,
+    w_r,
+    az_s,
+    az_r,
+    ax_s,
+    ax_r,
+    af_s,
+    af_r,
+    ac_s,
+    ac_r,
+    d_s,
+    d_r,
+    r1_s,
+    r1_r,
+    r2_s,
+    r2_r,
+    z_s,
+    z_r,
+):
+    ep, tp = lax.axis_index("ep"), lax.axis_index("tp")
+    rows, part = xbuf.shape[3], xbuf.shape[4]
+    half = rows // 2
+    width = 4 * part
+
+    def dev(zc, r):
+        return (lax.bitwise_xor(ep, zc), lax.bitwise_xor(tp, r))
+
+    def remote(src, dst, s_sem, r_sem, zc, r):
+        return pltpu.make_async_remote_copy(
+            src_ref=src,
+            dst_ref=dst,
+            send_sem=s_sem,
+            recv_sem=r_sem,
+            device_id=dev(zc, r),
+            device_id_type=MESH,
+        )
+
+    def quarter(r):
+        return pl.ds(pl.multiple_of(lax.bitwise_xor(tp, r) * part, part), part)
+
+    local = [pltpu.make_async_copy(tok_ref, xbuf.at[0, 0, 0], lsem.at[0])]
+    for r in range(4):
+        here = pl.ds(r * part, part)
+        local.append(pltpu.make_async_copy(gw_ref.at[0, quarter(r)], gw.at[here], lsem.at[1 + r]))
+        local.append(pltpu.make_async_copy(uw_ref.at[0, quarter(r)], uw.at[here], lsem.at[5 + r]))
+    local.append(pltpu.make_async_copy(dw_ref.at[0, quarter(0)], wd.at[0], lsem.at[9]))
+    for copy in local:
+        copy.start()
+
+    barrier = pltpu.get_barrier_semaphore()
+    for zc in range(1, 2 * nz):
+        pl.semaphore_signal(barrier, inc=1, device_id=dev(zc, 0), device_id_type=MESH)
+    for r in range(1, 4):
+        pl.semaphore_signal(barrier, inc=1, device_id=dev(0, r), device_id_type=MESH)
+
+    lane = lax.broadcasted_iota(jnp.int32, (rows, 128), 1)
+    dense = jnp.zeros((rows, 128), jnp.float32)
+    for k in range(ids_ref.shape[1]):
+        dense = dense + jnp.where(ids_ref[:, k : k + 1] == lane, route_ref[:, k : k + 1], 0.0)
+    wbuf[0] = dense.T[: 2 * nz]
+
+    local[0].wait()
+    pl.semaphore_wait(barrier, 2 * nz + 2)
+
+    started = []
+
+    def go(copy):
+        copy.start()
+        started.append(copy)
+        return copy
+
+    az = {}
+    for s in range(1, nz):
+        az[s] = go(remote(xbuf.at[0, 0, 0], xbuf.at[s, 0, 0], az_s.at[s], az_r.at[s], 2 * s, 0))
+    ax, af, ac = {}, {}, {}
+
+    def spread(s):
+        for r in (1, 2):
+            ax[s, r] = go(
+                remote(xbuf.at[s, 0, 0], xbuf.at[s, 0, r], ax_s.at[s, r], ax_r.at[s, r], 0, r)
+            )
+        share(s, 0)
+
+    def share(s, r):
+        ac[s, r] = go(
+            remote(xbuf.at[s, 0, r], xbuf.at[s, 1, r], ac_s.at[s, r], ac_r.at[s, r], 1, 0)
+        )
+
+    def pass_on(s):
+        for r, to in ((1, 2), (2, 1)):
+            ax[s, r].wait_recv()
+            piece = pl.ds((r - 1) * half, half)
+            af[s, r] = go(
+                remote(
+                    xbuf.at[s, 0, r, piece],
+                    xbuf.at[s, 0, 3, piece],
+                    af_s.at[s, r],
+                    af_r.at[s, r],
+                    0,
+                    to,
+                )
+            )
+            share(s, r)
+
+    def finish_gather(s):
+        af[s, 1].wait_recv()
+        af[s, 2].wait_recv()
+        share(s, 3)
+        for r in range(4):
+            ac[s, r].wait_recv()
+
+    spread(0)
+    w_copies = [
+        go(remote(wbuf.at[0], wbuf.at[zc], w_s.at[zc], w_r.at[zc], zc, 0))
+        for zc in range(1, 2 * nz)
+    ]
+    wd_copies = [
+        go(
+            remote(dw_ref.at[0, quarter(r)], wd.at[r], wd_s.at[r], wd_r.at[r], 0, r)
+        )
+        for r in range(1, 4)
+    ]
+
+    def compute(s):
+        for cr in range(2):
+            parts = [xbuf[s, cr, r].astype(jnp.float32) for r in range(4)]
+            square = parts[0] * parts[0]
+            for p in parts[1:]:
+                square = square + p * p
+            scale = lax.rsqrt(jnp.sum(square, axis=-1, keepdims=True) / width + epsilon)
+            for r in range(4):
+                gain = gain_ref[pl.ds(lax.bitwise_xor(tp, r), 1), :]
+                nbuf[pl.ds(cr * rows, rows), pl.ds(r * part, part)] = (
+                    parts[r] * scale * gain
+                ).astype(jnp.bfloat16)
+        g = jnp.dot(nbuf[...], gw[...], preferred_element_type=jnp.float32)
+        u = jnp.dot(nbuf[...], uw[...], preferred_element_type=jnp.float32)
+        g = jnp.minimum(g, clamp_limit)
+        u = jnp.clip(u, -clamp_limit, clamp_limit)
+        return ((u + 1.0) * g * jax.nn.sigmoid(swish_alpha * g)).astype(jnp.bfloat16)
+
+    def down(s, hidden):
+        scales = []
+        for cr in range(2):
+            line = wbuf[2 * s + cr, pl.ds(ep, 1), :]
+            column = jnp.broadcast_to(line, (rows, rows)).T
+            scales.append(jnp.concatenate([column] * (part // rows), axis=1))
+        for r in range(4):
+            full = jnp.dot(hidden, wd[r], preferred_element_type=jnp.float32)
+            keep[s, r] = full[:rows] * scales[0]
+            dsend[s, r] = full[rows:] * scales[1]
+        return go(remote(dsend.at[s], drecv.at[s], d_s.at[s], d_r.at[s], 1, 0))
+
+    d, r1, r2, zc_copies = {}, {}, {}, {}
+
+    def reduce_one(s):
+        d[s].wait_recv()
+        total = [keep[s, r] + drecv[s, r] for r in range(4)]
+        r1send[s, 0, 0] = total[1][:half].astype(jnp.bfloat16)
+        r1send[s, 0, 1] = total[3][:half].astype(jnp.bfloat16)
+        r1send[s, 1, 0] = total[2][half:].astype(jnp.bfloat16)
+        r1send[s, 1, 1] = total[3][half:].astype(jnp.bfloat16)
+        for h in range(2):
+            r1[s, h] = go(
+                remote(r1send.at[s, h], r1recv.at[s, h], r1_s.at[s, h], r1_r.at[s, h], 0, 1 + h)
+            )
+        keep[s, 0] = total[0]
+        keep[s, 1, half:] = total[1][half:]
+        keep[s, 2, :half] = total[2][:half]
+
+    def reduce_two(s):
+        for h in range(2):
+            r1[s, h].wait_recv()
+            piece = pl.ds(h * half, half)
+            r2send[s, h] = keep[s, 2 - h, piece] + r1recv[s, h, 1].astype(jnp.float32)
+            r2[s, h] = go(
+                remote(r2send.at[s, h], r2recv.at[s, h], r2_s.at[s, h], r2_r.at[s, h], 0, 2 - h)
+            )
+
+    def reduce_three(s):
+        for h in range(2):
+            r2[s, h].wait_recv()
+            piece = pl.ds(h * half, half)
+            value = (
+                keep[s, 0, piece]
+                + r1recv[s, h, 0].astype(jnp.float32)
+                + r2recv[s, h]
+            )
+            if s == 0:
+                keep[s, 0, piece] = value
+            elif s == 1:
+                near[0, piece] = value
+            else:
+                zsend[s, piece] = value.astype(jnp.bfloat16)
+        if s:
+            out, into = (near.at[0], near.at[1]) if s == 1 else (zsend.at[s], zrecv.at[s])
+            zc_copies[s] = go(remote(out, into, z_s.at[s], z_r.at[s], 2 * s, 0))
+
+    for s in range(nz):
+        if s + 1 < nz:
+            az[s + 1].wait_recv()
+            spread(s + 1)
+        pass_on(s)
+        finish_gather(s)
+        if s == 0:
+            for copy in local[1:]:
+                copy.wait()
+        hidden = compute(s)
+        if s == 0:
+            for copy in wd_copies + w_copies:
+                copy.wait_recv()
+        d[s] = down(s, hidden)
+        if s >= 1:
+            reduce_one(s - 1)
+        if s >= 2:
+            reduce_two(s - 2)
+        if s >= 3:
+            reduce_three(s - 3)
+    for s in range(nz, nz + 3):
+        if s - 1 < nz:
+            reduce_one(s - 1)
+        if 0 <= s - 2 < nz:
+            reduce_two(s - 2)
+        if 0 <= s - 3 < nz:
+            reduce_three(s - 3)
+    result = keep[0, 0]
+    for s in range(1, nz):
+        zc_copies[s].wait_recv()
+        result = result + (near[1] if s == 1 else zrecv[s].astype(jnp.float32))
+    out_ref[...] = result.astype(jnp.bfloat16)
+    for copy in started:
+        copy.wait_send()
+
+
+def fused_body(
+    nz, tokens, norm_gain, gate_weight, up_weight, down_weight, expert_ids, route_weight
+):
+    rows, part = tokens.shape
+    half = rows // 2
+    width = gate_weight.shape[1]
+    units = gate_weight.shape[2]
+    dma = pltpu.SemaphoreType.DMA
+    vmem = pl.BlockSpec(memory_space=pltpu.VMEM)
+    anywhere = pl.BlockSpec(memory_space=pl.ANY)
+    bf, f32 = jnp.bfloat16, jnp.float32
+    return pl.pallas_call(
+        functools.partial(fused_kernel, nz),
+        out_shape=jax.ShapeDtypeStruct((rows, part), bf),
+        in_specs=[vmem] * 3 + [anywhere] * 4,
+        out_specs=vmem,
+        scratch_shapes=[
+            pltpu.VMEM((nz, 2, 4, rows, part), bf),
+            pltpu.VMEM((width, units), bf),
+            pltpu.VMEM((width, units), bf),
+            pltpu.VMEM((4, units, part), bf),
+            pltpu.VMEM((2 * rows, width), bf),
+            pltpu.VMEM((2 * nz, 2 * nz, rows), f32),
+            pltpu.VMEM((nz, 4, rows, part), f32),
+            pltpu.VMEM((nz, 4, rows, part), f32),
+            pltpu.VMEM((nz, 4, rows, part), f32),
+            pltpu.VMEM((nz, 2, 2, half, part), bf),
+            pltpu.VMEM((nz, 2, 2, half, part), bf),
+            pltpu.VMEM((nz, 2, half, part), f32),
+            pltpu.VMEM((nz, 2, half, part), f32),
+            pltpu.VMEM((nz, rows, part), bf),
+            pltpu.VMEM((nz, rows, part), bf),
+            pltpu.VMEM((2, rows, part), f32),
+            dma((10,)),
+            dma((4,)),
+            dma((4,)),
+            dma((2 * nz,)),
+            dma((2 * nz,)),
+            dma((nz,)),
+            dma((nz,)),
+            dma((nz, 3)),
+            dma((nz, 3)),
+            dma((nz, 3)),
+            dma((nz, 3)),
+            dma((nz, 4)),
+            dma((nz, 4)),
+            dma((nz,)),
+            dma((nz,)),
+            dma((nz, 2)),
+            dma((nz, 2)),
+            dma((nz, 2)),
+            dma((nz, 2)),
+            dma((nz,)),
+            dma((nz,)),
+        ],
+        compiler_params=pltpu.CompilerParams(
+            collective_id=0, has_side_effects=True, vmem_limit_bytes=48 * 1024 * 1024
+        ),
+    )(
+        norm_gain.reshape(4, part),
+        expert_ids,
+        route_weight,
+        tokens,
+        gate_weight,
+        up_weight,
+        down_weight,
+    )
+
+
+def chosen(tokens, norm_gain, gate_weight, up_weight, down_weight, expert_ids, route_weight):
+    args = (tokens, norm_gain, gate_weight, up_weight, down_weight, expert_ids, route_weight)
+    ep_count, tp_count = lax.axis_size("ep"), lax.axis_size("tp")
+    rows, part = tokens.shape
+    units = gate_weight.shape[2]
+    nz = ep_count // 2
+    fits = (
+        tp_count == 4
+        and nz >= 2
+        and nz & (nz - 1) == 0
+        and nz <= 4
+        and ep_count % 8 == 0
+        and gate_weight.shape[0] == 1
+        and rows == 128
+        and part % 128 == 0
+        and units == part
+        and down_weight.shape[2] == part
+    )
+    if not fits:
+        return body(*args)
+    return fused_body(nz, *args)
+
+
 def solution(mesh):
     in_specs = (
         P("ep", "tp"),
@@ -99,4 +461,4 @@
         P("ep", None),
     )
     out_specs = P("ep", "tp")
-    return jax.shard_map(body, mesh=mesh, in_specs=in_specs, out_specs=out_specs, check_vma=False)
+    return jax.shard_map(chosen, mesh=mesh, in_specs=in_specs, out_specs=out_specs, check_vma=False)

time: 170 us -> 61.5 us (0.36)
  blocking collectives: 65.3 us -> 0 us
  Pallas kernels: 0 us -> 55.8 us
  waiting for transfers between devices: 48.3 us -> 0 us
  local copies, waits for them, and re-layouts: 30.1 us -> 5.32 us
  between operations: 13.5 us -> 0.02 us
  matrix products: 5.44 us -> 0 us
  starting transfers between devices: 4.61 us -> 0 us
  other arithmetic: 2.63 us -> 0 us
    pallas_call x0 -> x1, Pallas kernels: none -> 55.8 us  [fused_body(): pl.pallas_call(functools.partial(fused_kernel, nz), out_shape=jax.ShapeDt...]
    all_to_all x1 -> x0, blocking collectives: 53.8 us -> none  [body(): lax.all_to_all(outgoing, 'ep', split_axis=0, concat_axis=0, tiled=True)]
    all_gather x1 -> x0, waiting for transfers between devices: 33 us -> none  [over_all(): lax.all_gather(part, axis, axis=dim, tiled=True)]
    scatter x1 -> x0, local copies, waits for them, and re-layouts: 22.1 us -> none  [body(): slot_table = jnp.full((expert_total, capacity), tok_rows, jnp.int32).at[f...]
    all_to_all x1 -> x0, waiting for transfers between devices: 15.3 us -> none  [body(): lax.all_to_all(sendback, 'ep', split_axis=0, concat_axis=0, tiled=True)]
    all_gather x1 -> x0, blocking collectives: 11.6 us -> none  [body(): whole = lax.all_gather(tokens, 'tp', axis=1, tiled=True)]
    gather x2 -> x0, local copies, waits for them, and re-layouts: 6.01 us -> none  [the longest x1 4.07 us: body(): padded[slot_table.reshape(-1)].reshape(expert_total, capacity, width)]
    dot_general x3 -> x0, matrix products: 5.44 us -> none  [the longest x1 3.1 us: add_hidden(): jnp.einsum('esf,efd->esd', piece, down_rows, preferred_element_type=jnp.f...]
  transfers between devices with their start and end apart: 2 -> 0, of which waited for: 2 -> 0; matrix products, arithmetic and copies ran while one was open for 0% -> 0% of each run, Pallas kernels for 0% -> 0%
where the time goes in v1:
time: 61.5 us; the launch traced here: 61.1 us
  Pallas kernels  55.8 us (91%)
  local copies, waits for them, and re-layouts  5.32 us (9%)
    pallas_call x1, Pallas kernels, fused_body(): pl.pallas_call(functools.partial(fused_kernel, nz), out_shape=jax.ShapeDt...  55.8 us
    unnamed x15, local copies, waits for them, and re-layouts  4.61 us

profile of v1, /device:TPU:0, one launch (start us, length us, event | category | flops | bytes accessed | tf_op | source)
XLA Modules:
  0.0 61.1 jit_solution(17452274520624049094)
XLA Ops:
  0.0 0.0 copy-start.4
  0.0 0.7 %reshape.3.gain_ref = f32[4,256]{1,0:T(4,128)S(1)} reshape(f32[1024]{0:T(1024)} %param.8) | data formatting | bytes 8192 | tf_op jit(solution)/shard_map/reshape | solution.py:420
  0.7 0.0 copy-done.4
  0.7 0.0 copy-start.5
  0.7 0.0 copy-start.3
  0.7 0.1 copy.8.ids_ref
  0.8 0.6 copy-done.5
  1.4 0.1 copy.9.route_ref
  1.5 0.1 copy-done.3
  1.6 0.0 copy-start
  1.6 1.0 %copy-done = bf16[1,1024,256]{2,1,0:T(8,128)(2,1)S(1)} copy-done((bf16[1,1024,256]{2,1,0:T(8,128)(2,1)S(1)}, bf16[1,1024,256]{2,1,0:T(8,128)(2,1)}, u32[]{:S(2)}) %copy-start) | copy-done | bytes 524312
  2.6 0.0 copy-start.1
  2.6 1.0 %copy-done.1 = bf16[1,1024,256]{2,1,0:T(8,128)(2,1)S(1)} copy-done((bf16[1,1024,256]{2,1,0:T(8,128)(2,1)S(1)}, bf16[1,1024,256]{2,1,0:T(8,128)(2,1)}, u32[]{:S(2)}) %copy-start.1) | copy-done | bytes 524312
  3.7 0.0 copy-start.2
  3.7 1.0 %copy-done.2 = bf16[1,1024,256]{2,1,0:T(8,128)(2,1)S(1)} copy-done((bf16[1,1024,256]{2,1,0:T(8,128)(2,1)S(1)}, bf16[1,1024,256]{2,1,0:T(8,128)(2,1)}, u32[]{:S(2)}) %copy-start.2) | copy-done | bytes 524312
  4.7 55.8 %shard_map.73 = bf16[128,256]{1,0:T(8,128)(2,1)S(1)} custom-call(f32[4,256]{1,0:T(4,128)S(1)} %reshape.3.gain_ref, s32[128,4]{1,0:T(8,128)S(1)} %copy.8.ids_ref, f32[128,4]{1,0:T(8,128)S(1)} %copy.9.route_ref, bf16[128,256]{1,0:T(8,128)(2,1)S(1)} %copy-done.3, bf16[1,1024,256]{2,1,0:T(8,128)(2,1)S(1)} %copy-done, bf16[1,1024,256]{2,1,0:T(8,128)(2,1)S(1)} %copy-done.1, ...), custom_call_target="tpu_custom_call" | custom-call | tf_op jit(solution)/shard_map/pallas_call | solution.py:372
  60.5 0.6 %copy.11 = bf16[128,256]{1,0:T(8,128)(2,1)} copy(bf16[128,256]{1,0:T(8,128)(2,1)S(1)} %shard_map.73) | data formatting | bytes 131072
Async XLA Ops:
  0.0 0.7 %copy-start.4 = (s32[128,4]{0,1:T(4,128)S(1)}, s32[128,4]{0,1:T(4,128)}, u32[]{:S(2)}) copy-start(s32[128,4]{0,1:T(4,128)} %param.12) | copy-start | bytes 6148
  0.7 0.7 %copy-start.5 = (f32[128,4]{0,1:T(4,128)S(1)}, f32[128,4]{0,1:T(4,128)}, u32[]{:S(2)}) copy-start(f32[128,4]{0,1:T(4,128)} %param.13) | copy-start | bytes 6148
  0.7 0.9 %copy-start.3 = (bf16[128,256]{1,0:T(8,128)(2,1)S(1)}, bf16[128,256]{1,0:T(8,128)(2,1)}, u32[]{:S(2)}) copy-start(bf16[128,256]{1,0:T(8,128)(2,1)} %tok_ref.1) | copy-start | bytes 196612
  1.6 1.0 %copy-start = (bf16[1,1024,256]{2,1,0:T(8,128)(2,1)S(1)}, bf16[1,1024,256]{2,1,0:T(8,128)(2,1)}, u32[]{:S(2)}) copy-start(bf16[1,1024,256]{2,1,0:T(8,128)(2,1)} %gw_ref.1) | copy-start | bytes 1572868
  2.6 1.0 %copy-start.1 = (bf16[1,1024,256]{2,1,0:T(8,128)(2,1)S(1)}, bf16[1,1024,256]{2,1,0:T(8,128)(2,1)}, u32[]{:S(2)}) copy-start(bf16[1,1024,256]{2,1,0:T(8,128)(2,1)} %uw_ref.1) | copy-start | bytes 1572868
  3.7 1.0 %copy-start.2 = (bf16[1,1024,256]{2,1,0:T(8,128)(2,1)S(1)}, bf16[1,1024,256]{2,1,0:T(8,128)(2,1)}, u32[]{:S(2)}) copy-start(bf16[1,1024,256]{2,1,0:T(8,128)(2,1)} %dw_ref.1) | copy-start | bytes 1572868
